TPU v7x, 32 devices: a whole 2x2x4 slice. The times are simulated.
32 devices in a mesh: kv: 4 (over z), tp: 8 (over y, x, core).
Axes of the slice: x: 2, y: 2, z: 4, core: 2. Of those that a mesh axis runs over, the one named last changes fastest.
Arguments:
- piece_tokens: bfloat16 [512, 2048], P('kv'), may hold values from -6 to 6
- dec_tokens: bfloat16 [8, 2048], P('kv'), may hold values from -6 to 6
- norm_gain: float32 [2048], replicated, may hold values from 0.1 to 1.9
- w_query_nope: bfloat16 [2048, 2048], P(None, 'tp'), may hold values from -0.125 to 0.125
- w_query_rope: bfloat16 [2048, 1024], P(None, 'tp'), may hold values from -0.125 to 0.125
- w_latent: bfloat16 [2048, 512], replicated, may hold values from -0.125 to 0.125
- w_key_rope: bfloat16 [2048, 64], replicated, may hold values from -0.125 to 0.125
- latent_gain: float32 [512], replicated, may hold values from 0.1 to 1.9
- w_key_up: bfloat16 [16, 128, 512], P('tp'), may hold values from -0.5 to 0.5
- w_value_up: bfloat16 [16, 512, 128], P('tp'), may hold values from -3 to 3
- w_out: bfloat16 [2048, 2048], P(None, 'tp'), may hold values from -0.25 to 0.25
- prompt_latent: bfloat16 [2048, 512], P('kv'), may hold values from -210 to 210
- prompt_rope: bfloat16 [2048, 64], P('kv'), may hold values from -6 to 6
- dec_latent: bfloat16 [8, 1024, 512], P('kv'), may hold values from -210 to 210
- dec_rope: bfloat16 [8, 1024, 64], P('kv'), may hold values from -6 to 6
- dec_lengths: int32 [8], P('kv'), may hold values from 1 to 1024, 4096 in all
Outputs:
- piece_out: bfloat16 [512, 2048], P('kv', 'tp')
- dec_out: bfloat16 [8, 2048], P('kv', 'tp')
Inputs may be any that keep to these rules, and one draw needn't show every extreme that they name: `dec_lengths`: every decoding sequence has at least one live cache slot, and some sequence has all 1024.
All inputs are finite; a program needn't handle non-finite values. No bound on the sum of `dec_lengths` on one device may be relied on, other than what follows from the above.
Results may differ from a plain program's by a relative error of at most 0.025.
Values may be sent and summed in bfloat16 or wider, within the bound.
No kernel may reach another device: no remote copies, remote signals or barrier semaphores. Data moves between devices by JAX's collectives and lax.ppermute only.
A program may use at most 128 MiB of HBM per device.

v0:
```python
import jax
import jax.numpy as jnp
from jax import lax
from jax.sharding import PartitionSpec as P

epsilon = 1e-06
rope_base = 10000.0
masked = -1e30


def normalize(values, gain_vec):
    mean_sq = jnp.mean(values * values, axis=-1, keepdims=True)
    return values * lax.rsqrt(mean_sq + epsilon) * gain_vec


def rotate(values, positions):
    half_dim = values.shape[-1] // 2
    frequency = rope_base ** (-jnp.arange(half_dim, dtype=jnp.float32) / half_dim)
    angles = (positions.astype(jnp.float32)[:, None] * frequency[None, :])[:, None, :]
    cosines = jnp.cos(angles)
    sine_values = jnp.sin(angles)
    front_half = values[..., :half_dim]
    back_half = values[..., half_dim:]
    return jnp.concatenate(
        [
            front_half * cosines - back_half * sine_values,
            front_half * sine_values + back_half * cosines,
        ],
        axis=-1,
    )


def rounded(values):
    return lax.optimization_barrier(values.astype(jnp.bfloat16)).astype(jnp.float32)


def project(
    tokens, positions, norm_gain, w_query_nope, w_query_rope, w_latent, w_key_rope, latent_gain
):
    row_count = tokens.shape[0]
    rope_dim = w_key_rope.shape[1]
    head_count = w_query_rope.shape[1] // rope_dim
    normed = normalize(tokens.astype(jnp.float32), norm_gain).astype(jnp.bfloat16)
    query_nope = jnp.dot(normed, w_query_nope, preferred_element_type=jnp.float32).astype(
        jnp.bfloat16
    )
    query_raw = jnp.dot(normed, w_query_rope, preferred_element_type=jnp.float32).reshape(
        row_count, head_count, rope_dim
    )
    query_rot = rotate(query_raw, positions).astype(jnp.bfloat16)
    latent = normalize(
        jnp.dot(normed, w_latent, preferred_element_type=jnp.float32), latent_gain
    ).astype(jnp.bfloat16)
    key_raw = jnp.dot(normed, w_key_rope, preferred_element_type=jnp.float32)[:, None, :]
    key_rot = rotate(key_raw, positions)[:, 0].astype(jnp.bfloat16)
    return (query_nope, query_rot, latent, key_rot)


def absorb(query_nope, w_key_up):
    head_count, nope_dim, _ = w_key_up.shape
    by_head = query_nope.reshape(query_nope.shape[0], head_count, nope_dim)
    return jnp.einsum("nhd,hdc->nhc", by_head, w_key_up, preferred_element_type=jnp.float32).astype(
        jnp.bfloat16
    )


def shards(
    piece_tokens,
    dec_tokens,
    norm_gain,
    w_query_nope,
    w_query_rope,
    w_latent,
    w_key_rope,
    latent_gain,
    w_key_up,
    w_value_up,
    w_out,
    prompt_latent,
    prompt_rope,
    dec_latent,
    dec_rope,
    dec_lengths,
):
    piece_rows = piece_tokens.shape[0]
    dec_rows = dec_tokens.shape[0]
    cached = prompt_latent.shape[0]
    head_count, latent_dim, value_dim = w_value_up.shape
    rope_dim = w_key_rope.shape[1]
    nope_width = w_query_nope.shape[1]
    score_scale = (w_key_up.shape[1] + rope_dim) ** (-0.5)
    block_index = lax.axis_index("kv")
    prompt_len = cached * lax.axis_size("kv")
    piece_offset = block_index * piece_rows
    positions = jnp.concatenate(
        [prompt_len + piece_offset + jnp.arange(piece_rows, dtype=jnp.int32), dec_lengths]
    )
    tokens = jnp.concatenate([piece_tokens, dec_tokens], axis=0)
    query_nope, query_rot, new_latent, new_rot = project(
        tokens, positions, norm_gain, w_query_nope, w_query_rope, w_latent, w_key_rope, latent_gain
    )
    key_latent = jnp.concatenate([prompt_latent, new_latent[:piece_rows]], axis=0)
    key_rot = jnp.concatenate([prompt_rope, new_rot[:piece_rows]], axis=0)
    column = jnp.arange(key_latent.shape[0], dtype=jnp.int32)
    key_place = piece_offset + column - cached
    rot_width = head_count * rope_dim
    piece_rot = query_rot[:piece_rows].reshape(piece_rows, rot_width)
    outgoing = jnp.concatenate([query_nope[:piece_rows], piece_rot], axis=1)
    shard_rows = lax.all_gather(outgoing, "kv", axis=0, tiled=True)
    row_count = shard_rows.shape[0]
    query_lat = absorb(shard_rows[:, :nope_width], w_key_up)
    query_rope = shard_rows[:, nope_width:].reshape(row_count, head_count, rope_dim)
    score_row_count = query_lat.shape[0]
    scores = (
        jnp.einsum("qhc,kc->qhk", query_lat, key_latent, preferred_element_type=jnp.float32)
        + jnp.einsum("qhr,kr->qhk", query_rope, key_rot, preferred_element_type=jnp.float32)
    ) * score_scale
    query_place = jnp.arange(score_row_count, dtype=jnp.int32)
    visible = (column[None, :] < cached) | (key_place[None, :] <= query_place[:, None])
    scores = jnp.where(visible[:, None, :], scores, masked)
    row_peak = lax.pmax(jnp.max(scores, axis=2).astype(jnp.bfloat16), "kv").astype(jnp.float32)
    weights = jnp.exp(scores - row_peak[:, :, None])
    weight_sum = jnp.sum(weights, axis=2)
    mixed_lat = jnp.einsum(
        "qhk,kc->qhc", weights.astype(jnp.bfloat16), key_latent, preferred_element_type=jnp.float32
    ).astype(jnp.bfloat16)
    partial_value = jnp.einsum(
        "qhc,hcv->qhv", mixed_lat, w_value_up, preferred_element_type=jnp.float32
    )
    all_rows = partial_value.shape[0]
    partial_value = rounded(partial_value).reshape(all_rows, head_count * value_dim)
    summed, denominator = (
        lax.psum_scatter(
            partial_value.astype(jnp.bfloat16), "kv", scatter_dimension=0, tiled=True
        ).astype(jnp.float32),
        lax.psum_scatter(
            weight_sum.astype(jnp.bfloat16), "kv", scatter_dimension=0, tiled=True
        ).astype(jnp.float32),
    )
    piece_attn = (
        summed.reshape(piece_rows, head_count, value_dim) / denominator[:, :, None]
    ).astype(jnp.bfloat16)
    dec_query = absorb(query_nope[piece_rows:], w_key_up)
    dec_rot = query_rot[piece_rows:]
    own_lat = new_latent[piece_rows:]
    own_rot = new_rot[piece_rows:]
    cache_scores = (
        jnp.einsum("bhc,bkc->bhk", dec_query, dec_latent, preferred_element_type=jnp.float32)
        + jnp.einsum("bhr,bkr->bhk", dec_rot, dec_rope, preferred_element_type=jnp.float32)
    ) * score_scale
    live_keys = (
        jnp.arange(dec_latent.shape[1], dtype=jnp.int32)[None, None, :] < dec_lengths[:, None, None]
    )
    cache_scores = jnp.where(live_keys, cache_scores, masked)
    own_scores = (
        jnp.einsum("bhc,bc->bh", dec_query, own_lat, preferred_element_type=jnp.float32)
        + jnp.einsum("bhr,br->bh", dec_rot, own_rot, preferred_element_type=jnp.float32)
    ) * score_scale
    dec_peak = jnp.maximum(jnp.max(cache_scores, axis=2), own_scores)
    cache_w = jnp.exp(cache_scores - dec_peak[:, :, None])
    own_w = jnp.exp(own_scores - dec_peak)
    dec_sum = jnp.sum(cache_w, axis=2) + own_w
    dec_mix = (
        jnp.einsum(
            "bhk,bkc->bhc",
            cache_w.astype(jnp.bfloat16),
            dec_latent,
            preferred_element_type=jnp.float32,
        )
        + rounded(own_w)[:, :, None] * own_lat.astype(jnp.float32)[:, None, :]
    ).astype(jnp.bfloat16)
    dec_value = rounded(
        jnp.einsum("bhc,hcv->bhv", dec_mix, w_value_up, preferred_element_type=jnp.float32)
    )
    dec_attn = (dec_value / dec_sum[:, :, None]).astype(jnp.bfloat16)
    attended = jnp.concatenate(
        [
            piece_attn.reshape(piece_rows, head_count * value_dim),
            dec_attn.reshape(dec_rows, head_count * value_dim),
        ],
        axis=0,
    )
    result = jnp.dot(
        lax.all_gather(attended, "tp", axis=1, tiled=True),
        w_out,
        preferred_element_type=jnp.float32,
    ).astype(jnp.bfloat16)
    return (result[:piece_rows], result[piece_rows:])


def solution(mesh):
    in_specs = (
        P("kv", None),
        P("kv", None),
        P(),
        P(None, "tp"),
        P(None, "tp"),
        P(),
        P(),
        P(),
        P("tp", None, None),
        P("tp", None, None),
        P(None, "tp"),
        P("kv", None),
        P("kv", None),
        P("kv", None, None),
        P("kv", None, None),
        P("kv"),
    )
    out_specs = (P("kv", "tp"), P("kv", "tp"))
    return jax.shard_map(shards, mesh=mesh, in_specs=in_specs, out_specs=out_specs, check_vma=False)
```

profile of v0, /device:TPU:0, one launch (start us, length us, event | category | flops | bytes accessed | tf_op | source)
XLA Modules:
  0.0 113.8 jit_solution(15459763306817569072)
XLA Ops:
  7.3 1.4 %fusion.16 = f32[130]{0:T(256)S(1)} fusion(bf16[2,2048]{1,0:T(2,128)(2,1)} %param.17, bf16[128,2048]{1,0:T(8,128)(2,1)} %param.16), kind=kLoop, calls=%fused_computation.19 | loop fusion | flops 1597310 | bytes 533000 | tf_op jit(solution)/shard_map/reduce_sum | solution.py:12
  8.7 1.9 %convolution_convert_fusion.3 = bf16[130,256]{1,0:T(8,128)(2,1)S(1)} fusion(bf16[2048,256]{1,0:T(8,128)(2,1)} %param.19, f32[2048]{0:T(1024)} %param.18, f32[130]{0:T(256)S(1)} %add_rsqrt_fusion.1, bf16[2,2048]{1,0:T(2,128)(2,1)} %param.17, bf16[128,2048]{1,0:T(8,128)(2,1)} %param.16), kind=kOutput, calls=%fused_computation.17 | convolution fusion | flops 138211840 | bytes 1656328 | tf_op jit(solution)/shard_map/dot_general | solution.py:44
  10.6 0.4 fusion.63
  11.0 0.1 reshape.229
  11.2 0.6 multiply_reduce_fusion
  11.8 0.3 copy-done.11
  12.1 0.4 convolution_bitcast_fusion
  12.6 0.3 multiply_cosine_fusion
  12.9 0.2 fusion.36
  13.1 0.1 multiply_convert_fusion
  13.3 0.3 subtract_convert_fusion
  13.6 0.2 pad_maximum_fusion.4
  13.8 0.1 copy.44
  13.9 0.1 copy.45
  14.0 16.3 %all_gather.6 = bf16[512,384]{1,0:T(8,128)(2,1)S(1)} all-gather(bf16[128,384]{1,0:T(8,128)(2,1)S(1)} %pad_maximum_fusion.2), channel_id=1, replica_groups=mesh['kv'=4,'tp'=8] {'kv'}, dimensions={0}, use_global_device_ids=true | all-gather | bytes 491520 | tf_op jit(solution)/shard_map/all_gather | solution.py:109
  30.3 0.8 copy.47
  31.1 0.2 fusion.9
  31.3 3.8 %fusion.3 = f32[512,2,640]{2,0,1:T(8,128)} fusion(bf16[2,128,512]{2,1,0:T(8,128)(2,1)S(1)} %copy-done.2, bf16[128,512]{1,0:T(8,128)(2,1)S(1)} %slice.76, bf16[512,512]{1,0:T(8,128)(2,1)} %param.27, bf16[512,384]{1,0:T(8,128)(2,1)S(1)} %all_gather.6), kind=kOutput, calls=%fused_computation.9 | convolution fusion | flops 807141376 | bytes 3801088 | tf_op jit(solution)/shard_map/qhc,kc->qhk/dot_general | solution.py:115
  35.1 4.2 %fusion.68 = (bf16[512,2]{0,1:T(2,128)(2,1)S(1)}, f32[512,2,640]{2,0,1:T(8,128)}) fusion(f32[512,2,640]{2,0,1:T(8,128)} %fusion.3, bf16[512,2,64]{0,2,1:T(8,128)(2,1)} %bitcast.72, bf16[128,64]{0,1:T(8,128)(2,1)S(1)} %fusion.40, bf16[512,64]{0,1:T(8,128)(2,1)} %param.28, pred[512,640]{1,0:T(8,128)(4,1)S(1)} %fusion.9), kind=kOutput, calls=%fused_computation.102 | convolution fusion | flops 86670336 | bytes 5785600 | tf_op jit(solution)/shard_map/qhr,kr->qhk/dot_general | solution.py:116
  39.3 12.4 %pmax.7 = bf16[512,2]{0,1:T(2,128)(2,1)S(1)} all-reduce(bf16[512,2]{0,1:T(2,128)(2,1)S(1)} %get-tuple-element.16), channel_id=1, replica_groups=mesh['kv'=4,'tp'=8] {'kv'}, use_global_device_ids=true, to_apply=%region_3.4 | all-reduce | flops 1024 | bytes 4096 | tf_op jit(solution)/shard_map/pmax | solution.py:121
  51.8 2.4 %fusion = bf16[512,2]{0,1:T(2,128)(2,1)S(1)} fusion(f32[512,2,640]{2,0,1:T(8,128)} %get-tuple-element.17, f32[512,2]{0,1:T(2,128)S(1)} %convert_element_type.109), kind=kLoop, calls=%fused_computation.2 | loop fusion | flops 1309696 | bytes 2627584 | tf_op jit(solution)/shard_map/reduce_sum | solution.py:123
  54.1 0.8 copy.61
  55.0 0.0 reduce-scatter.7.cloned.1.call-start
  55.0 3.8 %fusion.13 = bf16[512,2,128]{2,0,1:T(8,128)(2,1)} fusion(bf16[2,512,128]{2,1,0:T(8,128)(2,1)} %param.25, f32[512,2,640]{2,0,1:T(8,128)} %get-tuple-element.17, f32[512,2]{0,1:T(2,128)S(1)} %convert_element_type.109, bf16[128,512]{1,0:T(8,128)(2,1)S(1)} %slice.76, bf16[512,512]{1,0:T(8,128)(2,1)S(1)} %copy-done.4), kind=kOutput, calls=%fused_computation.15 | convolution fusion | flops 808583168 | bytes 3805184 | tf_op jit(solution)/shard_map/qhc,hcv->qhv/dot_general | solution.py:127
  58.9 1.1 copy.48
  59.9 0.8 copy.59
  60.8 0.9 fusion.22
  61.7 0.2 pad_maximum_fusion.3
  61.9 0.1 iota_compare_fusion.1
  62.0 2.2 %fusion.49 = f32[2,2,1024]{2,1,0:T(2,128)S(1)} fusion(bf16[2,1024,512]{2,1,0:T(8,128)(2,1)} %param.29, bf16[2,2,512]{2,0,1:T(2,128)(2,1)S(1)} %fusion.22), kind=kOutput, calls=%fused_computation.77 | convolution fusion | flops 4194304 | bytes 2117632 | tf_op jit(solution)/shard_map/bhc,bkc->bhk/dot_general | solution.py:148
  64.2 0.1 fusion.46
  64.3 0.1 copy.51
  64.4 0.1 fusion.53
  64.5 0.3 fusion.67
  64.8 0.2 fusion.41
  65.0 2.0 %fusion.21 = bf16[2,2,512]{2,1,0:T(2,128)(2,1)S(1)} fusion(bf16[2,1024,512]{2,1,0:T(8,128)(2,1)} %param.29, f32[2,2,1024]{2,1,0:T(2,128)S(1)} %get-tuple-element.13, f32[2,2]{1,0:T(2,128)S(1)} %fusion.55, f32[2,512]{1,0:T(2,128)S(1)} %get-tuple-element.6, f32[2,2]{1,0:T(2,128)S(1)} %convert_element_type.123), kind=kOutput, calls=%fused_computation.26 | convolution fusion | flops 4208640 | bytes 2121760 | tf_op jit(solution)/shard_map/bhk,bkc->bhc/dot_general | solution.py:164
  67.0 0.1 fusion.23
  67.2 0.1 copy.53
  67.3 0.1 fusion.52
  67.4 0.1 copy.54
  67.5 5.3 %reduce-scatter.9.cloned.1.call-done = bf16[128,2]{1,0:T(8,128)(2,1)} async-done(((bf16[512,2]{1,0:T(8,128)(2,1)}), bf16[128,2]{1,0:T(8,128)(2,1)}) %reduce-scatter.9.cloned.1.call-update) | async-done | bytes 528
  72.8 0.8 copy.62
  73.6 19.7 %reduce-scatter.7.cloned.1.call-done = bf16[128,256]{1,0:T(8,128)(2,1)} async-done(((bf16[512,256]{1,0:T(8,128)(2,1)}), bf16[128,256]{1,0:T(8,128)(2,1)}) %reduce-scatter.7.cloned.1.call-update) | async-done | bytes 65552
  93.3 0.9 copy.60
  94.3 10.9 %all_gather.7 = bf16[130,2048]{0,1:T(8,128)(2,1)S(1)} all-gather(bf16[130,256]{0,1:T(8,128)(2,1)S(1)} %pad_maximum_fusion.1), channel_id=1, replica_groups=mesh['kv'=4,'tp'=8] {'tp'}, dimensions={1}, use_global_device_ids=true | all-gather | bytes 599040 | tf_op jit(solution)/shard_map/all_gather | solution.py:184
  105.2 0.5 convolution_convert_fusion.2
  105.7 0.6 slice.84
  106.4 0.6 slice.85
  (51 shorter events, 0.3 us)
Async XLA Ops:
  7.2 4.0 %copy-start = (bf16[2048,512]{1,0:T(8,128)(2,1)S(1)}, bf16[2048,512]{1,0:T(8,128)(2,1)}, u32[]{:S(2)}) copy-start(bf16[2048,512]{1,0:T(8,128)(2,1)} %param.21) | copy-start | bytes 6291460
  7.2 65.6 %reduce-scatter.9.cloned.1.call-start = ((), (), s32[]{:S(2)}) async-start(), calls=%async_computation.3 | async-start | bytes 163840
  8.6 1.9 %copy-start.3 = (bf16[128,2048]{1,0:T(8,128)(2,1)S(1)}, bf16[128,2048]{1,0:T(8,128)(2,1)}, u32[]{:S(2)}) copy-start(bf16[128,2048]{1,0:T(8,128)(2,1)} %param.16) | copy-start | bytes 1572868
  8.7 1.9 %copy-start.7 = (bf16[2,2048]{1,0:T(2,128)(2,1)S(1)}, bf16[2,2048]{1,0:T(2,128)(2,1)}, u32[]{:S(2)}) copy-start(bf16[2,2048]{1,0:T(2,128)(2,1)} %param.17) | copy-start | bytes 24580
  8.7 1.9 %copy-start.10 = (bf16[2048,128]{1,0:T(8,128)(2,1)S(1)}, bf16[2048,128]{1,0:T(8,128)(2,1)}, u32[]{:S(2)}) copy-start(bf16[2048,128]{1,0:T(8,128)(2,1)} %param.20) | copy-start | bytes 1572868
  8.7 1.9 %copy-start.13 = (f32[2048]{0:T(1024)S(1)}, f32[2048]{0:T(1024)}, u32[]{:S(2)}) copy-start(f32[2048]{0:T(1024)} %param.18) | copy-start | bytes 24580
  10.6 3.4 %copy-start.6 = (bf16[130,256]{1,0:T(8,128)(2,1)}, bf16[130,256]{1,0:T(8,128)(2,1)S(1)}, u32[]{:S(2)}) copy-start(bf16[130,256]{1,0:T(8,128)(2,1)S(1)} %convolution_convert_fusion.3) | copy-start | bytes 199684
  11.2 1.0 copy-start.11
  11.8 0.8 copy-start.9
  11.8 1.3 %copy-start.8 = (f32[512]{0:T(512)S(1)}, f32[512]{0:T(512)}, u32[]{:S(2)}) copy-start(f32[512]{0:T(512)} %param.23) | copy-start | bytes 6148
  13.2 18.1 %copy-start.2 = (bf16[2,128,512]{2,1,0:T(8,128)(2,1)S(1)}, bf16[2,128,512]{2,1,0:T(8,128)(2,1)}, u32[]{:S(2)}) copy-start(bf16[2,128,512]{2,1,0:T(8,128)(2,1)} %param.24) | copy-start | bytes 786436
  51.7 3.3 %copy-start.4 = (bf16[512,512]{1,0:T(8,128)(2,1)S(1)}, bf16[512,512]{1,0:T(8,128)(2,1)}, u32[]{:S(2)}) copy-start(bf16[512,512]{1,0:T(8,128)(2,1)} %param.27) | copy-start | bytes 1572868
  55.0 38.3 %reduce-scatter.7.cloned.1.call-start = ((), (), s32[]{:S(2)}) async-start(), calls=%async_computation.2 | async-start | bytes 327680
  60.8 3.7 %copy-start.12 = (bf16[2,1024,64]{1,2,0:T(8,128)(2,1)S(1)}, bf16[2,1024,64]{1,2,0:T(8,128)(2,1)}, u32[]{:S(2)}) copy-start(bf16[2,1024,64]{1,2,0:T(8,128)(2,1)} %param.30) | copy-start | bytes 786436
  64.2 2.8 %copy-start.5 = (bf16[2,512,128]{2,1,0:T(8,128)(2,1)S(1)}, bf16[2,512,128]{2,1,0:T(8,128)(2,1)}, u32[]{:S(2)}) copy-start(bf16[2,512,128]{2,1,0:T(8,128)(2,1)} %param.25) | copy-start | bytes 786436
  67.0 38.2 %copy-start.1 = (bf16[2048,256]{1,0:T(8,128)(2,1)S(1)}, bf16[2048,256]{1,0:T(8,128)(2,1)}, u32[]{:S(2)}) copy-start(bf16[2048,256]{1,0:T(8,128)(2,1)} %param.26) | copy-start | bytes 3145732
Sparse Core Ops, SparseCore 0:
  55.1 17.6 reduce-scatter.8
  75.1 18.2 reduce-scatter.6
where the time goes:
time: 114 us
  blocking collectives  39.6 us (35%)
  waiting for transfers between devices  25 us (22%)
  matrix products  21.3 us (19%)
  between operations  14.4 us (13%)
  local copies, waits for them, and re-layouts  7.52 us (7%)
  other arithmetic  5.78 us (5%)
    unnamed x4, waiting for transfers between devices  25 us
    all_gather x1, blocking collectives, shards(): shard_rows = lax.all_gather(outgoing, 'kv', axis=0, tiled=True)  16.3 us
    pmax x1, blocking collectives, shards(): lax.pmax(jnp.max(scores, axis=2).astype(jnp.bfloat16), 'kv')  12.4 us
    all_gather x1, blocking collectives, shards(): lax.all_gather(attended, 'tp', axis=1, tiled=True)  10.9 us
    dot_general x1, matrix products, shards(): jnp.einsum('qhr,kr->qhk', query_rope, key_rot, preferred_element_type=jnp...  4.18 us
    dot_general x1, matrix products, shards(): jnp.einsum('qhc,hcv->qhv', mixed_lat, w_value_up, preferred_element_type=...  3.83 us
    dot_general x1, matrix products, shards(): jnp.einsum('qhc,kc->qhk', query_lat, key_latent, preferred_element_type=j...  3.79 us
    unnamed x32, local copies, waits for them, and re-layouts  3.78 us
  transfers between devices with their start and end apart: 2, of which 2 were waited for; matrix products, arithmetic and copies ran while one was open for 12% of the time, Pallas kernels for 0%

commit v1 on v0

--- a/solution.py
+++ b/solution.py
@@ -181,7 +181,7 @@
         axis=0,
     )
     result = jnp.dot(
-        lax.all_gather(attended, "tp", axis=1, tiled=True),
+        jnp.concatenate(lax.all_gather(attended, "tp"), axis=1),
         w_out,
         preferred_element_type=jnp.float32,
     ).astype(jnp.bfloat16)

time: 114 us -> 115 us (level)
  local copies, waits for them, and re-layouts: 7.52 us -> 8.92 us
    unnamed x32 -> x35, local copies, waits for them, and re-layouts: 3.78 us -> 5.08 us
where the time goes in v1:
time: 115 us; the launch traced here: 114 us
  blocking collectives  38.6 us (34%)
  waiting for transfers between devices  25.1 us (22%)
  matrix products  21.2 us (18%)
  between operations  14.5 us (13%)
  local copies, waits for them, and re-layouts  8.92 us (8%)
  other arithmetic  5.78 us (5%)
    unnamed x4, waiting for transfers between devices  25.1 us
    all_gather x1, blocking collectives, shards(): shard_rows = lax.all_gather(outgoing, 'kv', axis=0, tiled=True)  16.3 us
    pmax x1, blocking collectives, shards(): lax.pmax(jnp.max(scores, axis=2).astype(jnp.bfloat16), 'kv')  12.4 us
    all_gather x1, blocking collectives, shards(): lax.all_gather(attended, 'tp')  9.93 us
    unnamed x35, local copies, waits for them, and re-layouts  5.08 us
    dot_general x1, matrix products, shards(): jnp.einsum('qhr,kr->qhk', query_rope, key_rot, preferred_element_type=jnp...  4.18 us
    dot_general x1, matrix products, shards(): jnp.einsum('qhc,hcv->qhv', mixed_lat, w_value_up, preferred_element_type=...  3.83 us
    dot_general x1, matrix products, shards(): jnp.einsum('qhc,kc->qhk', query_lat, key_latent, preferred_element_type=j...  3.79 us
  transfers between devices with their start and end apart: 2, of which 2 were waited for; matrix products, arithmetic and copies ran while one was open for 12% of the time, Pallas kernels for 0%

profile of v1, /device:TPU:0, one launch (start us, length us, event | category | flops | bytes accessed | tf_op | source)
XLA Modules:
  0.0 114.2 jit_solution(14728561092773755807)
XLA Ops:
  7.3 1.4 %fusion.16 = f32[130]{0:T(256)S(1)} fusion(bf16[2,2048]{1,0:T(2,128)(2,1)} %param.17, bf16[128,2048]{1,0:T(8,128)(2,1)} %param.16), kind=kLoop, calls=%fused_computation.19 | loop fusion | flops 1597310 | bytes 533000 | tf_op jit(solution)/shard_map/reduce_sum | solution.py:12
  8.7 1.9 %convolution_convert_fusion.3 = bf16[130,256]{1,0:T(8,128)(2,1)S(1)} fusion(bf16[2048,256]{1,0:T(8,128)(2,1)} %param.19, f32[2048]{0:T(1024)} %param.18, f32[130]{0:T(256)S(1)} %add_rsqrt_fusion.1, bf16[2,2048]{1,0:T(2,128)(2,1)} %param.17, bf16[128,2048]{1,0:T(8,128)(2,1)} %param.16), kind=kOutput, calls=%fused_computation.17 | convolution fusion | flops 138211840 | bytes 1656328 | tf_op jit(solution)/shard_map/dot_general | solution.py:44
  10.6 0.4 fusion.63
  11.0 0.1 reshape.235
  11.2 0.6 multiply_reduce_fusion
  11.8 0.3 copy-done.11
  12.1 0.4 convolution_bitcast_fusion
  12.6 0.3 multiply_cosine_fusion
  12.9 0.2 fusion.36
  13.1 0.1 multiply_convert_fusion
  13.3 0.3 subtract_convert_fusion
  13.6 0.2 pad_maximum_fusion.3
  13.8 0.1 copy.46
  13.9 0.1 copy.47
  14.0 16.3 %all_gather.9 = bf16[512,384]{1,0:T(8,128)(2,1)S(1)} all-gather(bf16[128,384]{1,0:T(8,128)(2,1)S(1)} %pad_maximum_fusion.1), channel_id=1, replica_groups=mesh['kv'=4,'tp'=8] {'kv'}, dimensions={0}, use_global_device_ids=true | all-gather | bytes 491520 | tf_op jit(solution)/shard_map/all_gather | solution.py:109
  30.3 0.8 copy.49
  31.1 0.2 fusion.9
  31.3 3.8 %fusion.3 = f32[512,2,640]{2,0,1:T(8,128)} fusion(bf16[2,128,512]{2,1,0:T(8,128)(2,1)S(1)} %copy-done.2, bf16[128,512]{1,0:T(8,128)(2,1)S(1)} %slice.76, bf16[512,512]{1,0:T(8,128)(2,1)} %param.27, bf16[512,384]{1,0:T(8,128)(2,1)S(1)} %all_gather.9), kind=kOutput, calls=%fused_computation.9 | convolution fusion | flops 807141376 | bytes 3801088 | tf_op jit(solution)/shard_map/qhc,kc->qhk/dot_general | solution.py:115
  35.1 4.2 %fusion.68 = (bf16[512,2]{0,1:T(2,128)(2,1)S(1)}, f32[512,2,640]{2,0,1:T(8,128)}) fusion(f32[512,2,640]{2,0,1:T(8,128)} %fusion.3, bf16[512,2,64]{0,2,1:T(8,128)(2,1)} %bitcast.81, bf16[128,64]{0,1:T(8,128)(2,1)S(1)} %fusion.40, bf16[512,64]{0,1:T(8,128)(2,1)} %param.28, pred[512,640]{1,0:T(8,128)(4,1)S(1)} %fusion.9), kind=kOutput, calls=%fused_computation.102 | convolution fusion | flops 86670336 | bytes 5785600 | tf_op jit(solution)/shard_map/qhr,kr->qhk/dot_general | solution.py:116
  39.3 12.4 %pmax.7 = bf16[512,2]{0,1:T(2,128)(2,1)S(1)} all-reduce(bf16[512,2]{0,1:T(2,128)(2,1)S(1)} %get-tuple-element.16), channel_id=1, replica_groups=mesh['kv'=4,'tp'=8] {'kv'}, use_global_device_ids=true, to_apply=%region_3.4 | all-reduce | flops 1024 | bytes 4096 | tf_op jit(solution)/shard_map/pmax | solution.py:121
  51.8 2.4 %fusion = bf16[512,2]{0,1:T(2,128)(2,1)S(1)} fusion(f32[512,2,640]{2,0,1:T(8,128)} %get-tuple-element.17, f32[512,2]{0,1:T(2,128)S(1)} %convert_element_type.109), kind=kLoop, calls=%fused_computation.2 | loop fusion | flops 1309696 | bytes 2627584 | tf_op jit(solution)/shard_map/reduce_sum | solution.py:123
  54.1 0.8 copy.65
  55.0 3.8 %fusion.13 = bf16[512,2,128]{2,0,1:T(8,128)(2,1)} fusion(bf16[2,512,128]{2,1,0:T(8,128)(2,1)} %param.25, f32[512,2,640]{2,0,1:T(8,128)} %get-tuple-element.17, f32[512,2]{0,1:T(2,128)S(1)} %convert_element_type.109, bf16[128,512]{1,0:T(8,128)(2,1)S(1)} %slice.76, bf16[512,512]{1,0:T(8,128)(2,1)S(1)} %copy-done.4), kind=kOutput, calls=%fused_computation.15 | convolution fusion | flops 808583168 | bytes 3805184 | tf_op jit(solution)/shard_map/qhc,hcv->qhv/dot_general | solution.py:127
  58.9 1.1 copy.50
  59.9 0.8 copy.63
  60.8 0.9 fusion.22
  61.7 0.2 pad_maximum_fusion.2
  62.0 2.2 %fusion.49 = f32[2,2,1024]{2,1,0:T(2,128)S(1)} fusion(bf16[2,1024,512]{2,1,0:T(8,128)(2,1)} %param.29, bf16[2,2,512]{2,0,1:T(2,128)(2,1)S(1)} %fusion.22), kind=kOutput, calls=%fused_computation.77 | convolution fusion | flops 4194304 | bytes 2117632 | tf_op jit(solution)/shard_map/bhc,bkc->bhk/dot_general | solution.py:148
  64.2 0.1 fusion.46
  64.4 0.1 fusion.53
  64.5 0.3 fusion.67
  64.8 0.2 fusion.41
  65.0 2.0 %fusion.21 = bf16[2,2,512]{2,1,0:T(2,128)(2,1)S(1)} fusion(bf16[2,1024,512]{2,1,0:T(8,128)(2,1)} %param.29, f32[2,2,1024]{2,1,0:T(2,128)S(1)} %get-tuple-element.13, f32[2,2]{1,0:T(2,128)S(1)} %fusion.55, f32[2,512]{1,0:T(2,128)S(1)} %get-tuple-element.6, f32[2,2]{1,0:T(2,128)S(1)} %convert_element_type.123), kind=kOutput, calls=%fused_computation.26 | convolution fusion | flops 4208640 | bytes 2121760 | tf_op jit(solution)/shard_map/bhk,bkc->bhc/dot_general | solution.py:164
  67.0 0.2 fusion.23
  67.2 0.1 copy.55
  67.4 0.1 copy.56
  67.5 5.3 %reduce-scatter.9.cloned.1.call-done = bf16[128,2]{1,0:T(8,128)(2,1)} async-done(((bf16[512,2]{1,0:T(8,128)(2,1)}), bf16[128,2]{1,0:T(8,128)(2,1)}) %reduce-scatter.9.cloned.1.call-update) | async-done | bytes 528
  72.8 0.8 copy.66
  73.6 19.8 %reduce-scatter.7.cloned.1.call-done = bf16[128,256]{1,0:T(8,128)(2,1)} async-done(((bf16[512,256]{1,0:T(8,128)(2,1)}), bf16[128,256]{1,0:T(8,128)(2,1)}) %reduce-scatter.7.cloned.1.call-update) | async-done | bytes 65552
  93.4 0.9 copy.64
  94.4 0.1 copy.57
  94.5 9.9 %all-gather.1 = bf16[8,130,256]{2,1,0:T(8,128)(2,1)S(1)} all-gather(bf16[1,130,256]{2,1,0:T(8,128)(2,1)S(1)} %copy.57), channel_id=2, replica_groups=mesh['kv'=4,'tp'=8] {'tp'}, dimensions={0}, use_global_device_ids=true | all-gather | bytes 599040 | tf_op jit(solution)/shard_map/all_gather | solution.py:184
  104.5 0.1 copy.58
  104.6 0.1 copy.68
  104.8 1.0 copy-done.1
  105.8 0.3 convolution_convert_fusion.2
  106.1 0.6 slice.84
  106.8 0.6 slice.85
  (55 shorter events, 0.6 us)
Async XLA Ops:
  7.2 4.0 %copy-start = (bf16[2048,512]{1,0:T(8,128)(2,1)S(1)}, bf16[2048,512]{1,0:T(8,128)(2,1)}, u32[]{:S(2)}) copy-start(bf16[2048,512]{1,0:T(8,128)(2,1)} %param.21) | copy-start | bytes 6291460
  7.2 65.6 %reduce-scatter.9.cloned.1.call-start = ((), (), s32[]{:S(2)}) async-start(), calls=%async_computation.3 | async-start | bytes 163840
  8.6 1.9 %copy-start.3 = (bf16[128,2048]{1,0:T(8,128)(2,1)S(1)}, bf16[128,2048]{1,0:T(8,128)(2,1)}, u32[]{:S(2)}) copy-start(bf16[128,2048]{1,0:T(8,128)(2,1)} %param.16) | copy-start | bytes 1572868
  8.7 1.9 %copy-start.7 = (bf16[2,2048]{1,0:T(2,128)(2,1)S(1)}, bf16[2,2048]{1,0:T(2,128)(2,1)}, u32[]{:S(2)}) copy-start(bf16[2,2048]{1,0:T(2,128)(2,1)} %param.17) | copy-start | bytes 24580
  8.7 1.9 %copy-start.10 = (bf16[2048,128]{1,0:T(8,128)(2,1)S(1)}, bf16[2048,128]{1,0:T(8,128)(2,1)}, u32[]{:S(2)}) copy-start(bf16[2048,128]{1,0:T(8,128)(2,1)} %param.20) | copy-start | bytes 1572868
  8.7 1.9 %copy-start.13 = (f32[2048]{0:T(1024)S(1)}, f32[2048]{0:T(1024)}, u32[]{:S(2)}) copy-start(f32[2048]{0:T(1024)} %param.18) | copy-start | bytes 24580
  10.6 3.4 %copy-start.6 = (bf16[130,256]{1,0:T(8,128)(2,1)}, bf16[130,256]{1,0:T(8,128)(2,1)S(1)}, u32[]{:S(2)}) copy-start(bf16[130,256]{1,0:T(8,128)(2,1)S(1)} %convolution_convert_fusion.3) | copy-start | bytes 199684
  11.2 1.0 copy-start.11
  11.8 0.8 copy-start.9
  11.8 1.3 %copy-start.8 = (f32[512]{0:T(512)S(1)}, f32[512]{0:T(512)}, u32[]{:S(2)}) copy-start(f32[512]{0:T(512)} %param.23) | copy-start | bytes 6148
  13.2 18.1 %copy-start.2 = (bf16[2,128,512]{2,1,0:T(8,128)(2,1)S(1)}, bf16[2,128,512]{2,1,0:T(8,128)(2,1)}, u32[]{:S(2)}) copy-start(bf16[2,128,512]{2,1,0:T(8,128)(2,1)} %param.24) | copy-start | bytes 786436
  51.7 3.3 %copy-start.4 = (bf16[512,512]{1,0:T(8,128)(2,1)S(1)}, bf16[512,512]{1,0:T(8,128)(2,1)}, u32[]{:S(2)}) copy-start(bf16[512,512]{1,0:T(8,128)(2,1)} %param.27) | copy-start | bytes 1572868
  55.0 38.5 %reduce-scatter.7.cloned.1.call-start = ((), (), s32[]{:S(2)}) async-start(), calls=%async_computation.2 | async-start | bytes 327680
  60.8 3.7 %copy-start.12 = (bf16[2,1024,64]{1,2,0:T(8,128)(2,1)S(1)}, bf16[2,1024,64]{1,2,0:T(8,128)(2,1)}, u32[]{:S(2)}) copy-start(bf16[2,1024,64]{1,2,0:T(8,128)(2,1)} %param.30) | copy-start | bytes 786436
  64.2 2.8 %copy-start.5 = (bf16[2,512,128]{2,1,0:T(8,128)(2,1)S(1)}, bf16[2,512,128]{2,1,0:T(8,128)(2,1)}, u32[]{:S(2)}) copy-start(bf16[2,512,128]{2,1,0:T(8,128)(2,1)} %param.25) | copy-start | bytes 786436
  104.6 1.2 %copy-start.1 = (bf16[2048,256]{1,0:T(8,128)(2,1)S(1)}, bf16[2048,256]{1,0:T(8,128)(2,1)}, u32[]{:S(2)}) copy-start(bf16[2048,256]{1,0:T(8,128)(2,1)} %param.26) | copy-start | bytes 3145732
Sparse Core Ops, SparseCore 0:
  55.1 17.6 reduce-scatter.8
  75.1 18.3 reduce-scatter.6
